TPU v7x, 32 devices: a whole 2x2x4 slice. The times are simulated.
32 devices in a mesh: sp: 4 (over z), fs: 4 (over y, x), tp: 2 (over core).
Axes of the slice: x: 2, y: 2, z: 4, core: 2. Of those that a mesh axis runs over, the one named last changes fastest.
Arguments:
- tokens: bfloat16 [4096, 2048], P(('fs', 'sp')), parts along dimension 0, may hold values from -6 to 6
- norm_gain: float32 [2048], replicated, may hold values from 0.1 to 1.9
- w_query: bfloat16 [2048, 1024], P('sp', 'tp'), may hold values from -0.080939698 to 0.080939698
- w_key: bfloat16 [2048, 256], P('sp', 'tp'), may hold values from -0.080939698 to 0.080939698
- w_value: bfloat16 [2048, 256], P('sp', 'tp'), may hold values from -0.125 to 0.125
- w_conv_in: bfloat16 [2048, 1024], P('sp', 'tp'), may hold values from -0.125 to 0.125
- w_conv_gate: bfloat16 [2048, 1024], P('sp', 'tp'), may hold values from -0.125 to 0.125
- sink_logit: float32 [16], P('tp'), may hold values from 2 to 6
- conv_taps: float32 [31, 1024], P(None, 'tp'), may hold values from -5.3881591 to 5.3881591
- conv_bias: float32 [1024], P('tp'), may hold values from -0.9 to 5.9
- channel_gain: float32 [1024], P('tp'), may hold values from 0.1 to 1.9
- channel_shift: float32 [1024], P('tp'), may hold values from -3 to 3
- w_attn_out: bfloat16 [1024, 2048], P(None, 'sp'), may hold values from -1.5 to 1.5
- w_conv_out: bfloat16 [1024, 2048], P(None, 'sp'), may hold values from -0.1875 to 0.1875
Outputs:
- output: bfloat16 [4096, 2048], P(('fs', 'sp', 'tp')), parts along dimension 0
There are 4 independent parts, one for each index of `fs`. A program takes and returns all parts, laid end to end along the dimension named above; an argument that names none is the same for every part. Nothing has to cross between parts.
All inputs are finite; a program needn't handle non-finite values.
Results may differ from a plain program's by a relative error of at most 0.011.
Values may be sent and summed in bfloat16 or wider, within the bound.
A program may use at most 64 MiB of HBM per device.

v0:
```python
import jax
import jax.numpy as jnp
from jax import lax
from jax.sharding import PartitionSpec as P

HEAD_DIM = 64
WINDOW = 128
GRID_W = 64
EPSILON = 1e-06
NEGATIVE = -1e30
ROPE_BASE = 10000.0


def padded(block, sides, width):
    for axis, dim in sides:
        count = lax.axis_size(axis)
        forward = [(i, i + 1) for i in range(count - 1)]
        backward = [(target, source) for source, target in forward]
        low = lax.ppermute(
            lax.slice_in_dim(block, block.shape[dim] - width, None, axis=dim), axis, forward
        )
        high = lax.ppermute(lax.slice_in_dim(block, 0, width, axis=dim), axis, backward)
        block = jnp.concatenate([low, block, high], axis=dim)
    return block


def rotate_pairs(values, positions):
    middle = values.shape[-1] // 2
    inverse = ROPE_BASE ** (-jnp.arange(middle, dtype=jnp.float32) / middle)
    angles = positions.astype(jnp.float32)[:, None] * inverse[None, :]
    cosine = jnp.cos(angles)[:, None, :]
    sine_table = jnp.sin(angles)[:, None, :]
    leading = values[..., :middle]
    trailing = values[..., middle:]
    return jnp.concatenate(
        [leading * cosine - trailing * sine_table, leading * sine_table + trailing * cosine],
        axis=-1,
    )


def grid_rotate(values, positions):
    middle = values.shape[-1] // 2
    return jnp.concatenate(
        [
            rotate_pairs(values[..., :middle], positions // GRID_W),
            rotate_pairs(values[..., middle:], positions % GRID_W),
        ],
        axis=-1,
    )


def local(
    tokens,
    norm_gain,
    w_query,
    w_key,
    w_value,
    w_conv_in,
    w_conv_gate,
    sink_logit,
    conv_taps,
    conv_bias,
    channel_gain,
    channel_shift,
    w_attn_out,
    w_conv_out,
):
    rows_here = tokens.shape[0]
    offset = lax.axis_index("sp") * rows_here
    total = rows_here * lax.axis_size("sp")
    tp_count = lax.axis_size("tp")
    token_float = tokens.astype(jnp.float32)
    normed = (
        token_float
        * lax.rsqrt(jnp.mean(token_float * token_float, axis=-1, keepdims=True) + EPSILON)
        * norm_gain[None, :]
    ).astype(jnp.bfloat16)
    head_cols = w_query.shape[1]
    kv_cols = w_key.shape[1]
    chan_cols = w_conv_in.shape[1]
    piece_query = lax.all_gather(w_query, "sp", axis=0, tiled=True)
    piece_key = lax.all_gather(w_key, "sp", axis=0, tiled=True)
    piece_value = lax.all_gather(w_value, "sp", axis=0, tiled=True)
    piece_conv = lax.all_gather(w_conv_in, "sp", axis=0, tiled=True)
    piece_gate = lax.all_gather(w_conv_gate, "sp", axis=0, tiled=True)
    query_acc = jnp.dot(normed, piece_query, preferred_element_type=jnp.float32)
    pair_acc = jnp.dot(
        normed,
        jnp.concatenate([piece_key, piece_value], axis=1),
        preferred_element_type=jnp.float32,
    )
    conv_acc = jnp.dot(
        normed,
        jnp.concatenate([piece_conv, piece_gate], axis=1),
        preferred_element_type=jnp.float32,
    )
    positions = offset + jnp.arange(rows_here, dtype=jnp.int32)
    heads_here = head_cols // HEAD_DIM
    kv_here = kv_cols // HEAD_DIM
    group = heads_here // kv_here
    query = grid_rotate(query_acc.reshape(rows_here, heads_here, HEAD_DIM), positions).astype(
        jnp.bfloat16
    )
    keys = grid_rotate(pair_acc[:, :kv_cols].reshape(rows_here, kv_here, HEAD_DIM), positions)
    keys = keys.astype(jnp.bfloat16).reshape(rows_here, kv_cols)
    values = pair_acc[:, kv_cols:].astype(jnp.bfloat16)
    stacked = jnp.concatenate([keys, values], axis=1)
    extended = padded(stacked, (("sp", 0),), WINDOW)
    block = min(rows_here, 512)
    span = block + 2 * WINDOW
    sinks = sink_logit.reshape(kv_here, group)[:, :, None, None]
    queries = query.reshape(block, kv_here, group, HEAD_DIM)
    near_keys = extended[:, :kv_cols].reshape(span, kv_here, HEAD_DIM)
    near_values = extended[:, kv_cols:].reshape(span, kv_here, HEAD_DIM)
    scores = jnp.einsum(
        "qkgd,skd->kgqs", queries, near_keys, preferred_element_type=jnp.float32
    ) * HEAD_DIM ** (-0.5)
    query_pos = offset + 0 + jnp.arange(block, dtype=jnp.int32)
    key_pos = offset + 0 - WINDOW + jnp.arange(span, dtype=jnp.int32)
    valid = (
        (jnp.abs(query_pos[:, None] - key_pos[None, :]) <= WINDOW)
        & (key_pos[None, :] >= 0)
        & (key_pos[None, :] < total)
    )
    scores = jnp.where(valid[None, None], scores, NEGATIVE)
    top = jnp.maximum(jnp.max(scores, axis=-1, keepdims=True), sinks)
    raised = jnp.exp(scores - top)
    denominator = jnp.sum(raised, axis=-1, keepdims=True) + jnp.exp(sinks - top)
    probs = (raised / denominator).astype(jnp.bfloat16)
    mixed = jnp.einsum("kgqs,skd->qkgd", probs, near_values, preferred_element_type=jnp.float32)
    outputs = mixed.astype(jnp.bfloat16).reshape(block, head_cols)
    glu = (conv_acc[:, :chan_cols] * jax.nn.sigmoid(conv_acc[:, chan_cols:])).astype(jnp.bfloat16)
    reach = conv_taps.shape[0] // 2
    rims = padded(glu, (("sp", 0),), reach)
    filtered = jnp.zeros((rows_here, chan_cols), jnp.float32) + conv_bias[None, :]
    for shift_index in range(conv_taps.shape[0]):
        filtered = filtered + conv_taps[shift_index][None, :] * rims[
            shift_index : shift_index + rows_here
        ].astype(jnp.float32)
    channel_total = chan_cols * tp_count
    centre = lax.psum(jnp.sum(filtered, axis=-1), "tp")[:, None] / channel_total
    centred = filtered - centre
    spread = lax.psum(jnp.sum(centred * centred, axis=-1), "tp")[:, None] / channel_total
    conv_out = jax.nn.silu(
        centred * lax.rsqrt(spread + EPSILON) * channel_gain[None, :] + channel_shift[None, :]
    ).astype(jnp.bfloat16)
    features = jnp.concatenate([outputs, conv_out], axis=1)
    tp_here = lax.axis_index("tp")
    own_rows = jnp.concatenate(
        [
            lax.dynamic_slice_in_dim(w_attn_out, tp_here * head_cols, head_cols, 0),
            lax.dynamic_slice_in_dim(w_conv_out, tp_here * chan_cols, chan_cols, 0),
        ],
        axis=0,
    )
    own_whole = lax.all_gather(own_rows, "sp", axis=1, tiled=True)
    result = lax.psum_scatter(
        jnp.dot(features, own_whole, preferred_element_type=jnp.float32).astype(jnp.bfloat16),
        "tp",
        scatter_dimension=0,
        tiled=True,
    )
    return result


def solution(mesh):
    in_specs = (
        P(("fs", "sp"), None),
        P(),
        P("sp", "tp"),
        P("sp", "tp"),
        P("sp", "tp"),
        P("sp", "tp"),
        P("sp", "tp"),
        P("tp"),
        P(None, "tp"),
        P("tp"),
        P("tp"),
        P("tp"),
        P(None, "sp"),
        P(None, "sp"),
    )
    out_specs = P(("fs", "sp", "tp"), None)
    return jax.shard_map(local, mesh=mesh, in_specs=in_specs, out_specs=out_specs, check_vma=False)
```

profile of v0, /device:TPU:0, one launch (start us, length us, event | category | flops | bytes accessed | tf_op | source)
XLA Modules:
  0.0 263.5 jit_solution(13735289390232705822)
XLA Ops:
  6.5 0.7 all-gather.7.cloned.1.call-update
  7.3 0.7 all-gather.9.cloned.1.call-update
  8.1 0.7 all-gather.5.cloned.1.call-update
  8.8 1.3 constant_dynamic-slice_fusion
  10.1 1.0 pad_maximum_fusion
  11.3 0.3 fusion.6
  11.6 23.1 %all_gather.18 = bf16[2048,128]{1,0:T(8,128)(2,1)S(1)} all-gather(bf16[512,128]{1,0:T(8,128)(2,1)S(1)} %copy-done.1), channel_id=1, replica_groups=mesh['sp'=4,'fs'=4,'tp'=2] {'sp'}, dimensions={0}, use_global_device_ids=true | all-gather | bytes 655360 | tf_op jit(solution)/shard_map/all_gather | solution.py:82
  34.7 21.7 %all_gather.19 = bf16[2048,128]{1,0:T(8,128)(2,1)S(1)} all-gather(bf16[512,128]{1,0:T(8,128)(2,1)S(1)} %copy-done.2), channel_id=1, replica_groups=mesh['sp'=4,'fs'=4,'tp'=2] {'sp'}, dimensions={0}, use_global_device_ids=true | all-gather | bytes 655360 | tf_op jit(solution)/shard_map/all_gather | solution.py:83
  56.4 0.7 fusion.11
  57.4 1.5 collective-permute-start
  58.9 1.3 collective-permute-start.1
  60.3 0.3 fusion.24
  60.7 1.5 collective-permute-done
  62.2 7.0 %collective-permute-done.1 = bf16[128,256]{0,1:T(8,128)(2,1)S(1)} collective-permute-done((bf16[128,256]{0,1:T(8,128)(2,1)S(1)}, bf16[128,256]{0,1:T(8,128)(2,1)S(1)}, u32[]{:S(2)}, u32[]{:S(2)}) %collective-permute-start.1) | collective-permute-done | bytes 65568 | tf_op jit(solution)/shard_map/ppermute | solution.py:22
  69.2 1.9 all-gather.7.cloned.1.call-done
  71.1 47.3 %all-gather.9.cloned.1.call-done = bf16[2048,512]{1,0:T(8,128)(2,1)} async-done(((bf16[512,512]{1,0:T(8,128)(2,1)}), bf16[2048,512]{1,0:T(8,128)(2,1)}) %all-gather.9.cloned.1.call-update) | async-done | bytes 2097168 | tf_op jit(solution)/shard_map/all_gather | solution.py:85
  118.4 3.5 %fusion = f32[256,1024]{1,0:T(8,128)S(1)} fusion(bf16[2048,512]{1,0:T(8,128)(2,1)} %all-gather.9.cloned.1.call-done, bf16[2048,512]{1,0:T(8,128)(2,1)} %all-gather.7.cloned.1.call-done, bf16[256,2048]{1,0:T(8,128)(2,1)S(1)} %copy-done, f32[2048]{0:T(1024)S(1)} %copy-done.7, f32[256]{0:T(256)S(1)} %add_rsqrt_fusion.1), kind=kOutput, calls=%fused_computation | convolution fusion | flops 1084227584 | bytes 6300672 | tf_op jit(solution)/shard_map/dot_general | solution.py:92
  122.1 2.1 collective-permute-start.2
  124.2 1.3 collective-permute-start.3
  125.5 39.2 %all-gather.5.cloned.1.call-done = bf16[2048,512]{1,0:T(8,128)(2,1)} async-done(((bf16[512,512]{1,0:T(8,128)(2,1)}), bf16[2048,512]{1,0:T(8,128)(2,1)}) %all-gather.5.cloned.1.call-update) | async-done | bytes 2097168 | tf_op jit(solution)/shard_map/all_gather | solution.py:81
  164.6 2.6 fusion.74
  167.3 0.8 fusion.5
  168.2 0.9 fusion.4
  169.3 1.2 fusion.10
  170.7 3.1 %fusion.77 = (f32[256]{0:T(256)S(1)}, f32[256,512]{1,0:T(8,128)S(1)}) fusion(bf16[15,512]{1,0:T(8,128)(2,1)S(1)} %collective-permute-done.3, bf16[256,512]{1,0:T(8,128)(2,1)S(1)} %fusion.22, f32[512]{0:T(512)S(1)} %bitcast.106, f32[512]{0:T(512)S(1)} %bitcast.107, f32[512]{0:T(512)S(1)} %bitcast.78, f32[512]{0:T(512)S(1)} %bitcast.79, f32[512]{0:T(512)S(1)} %bitcast.80, ...), kind=kLoop, calls=%fused_computation.167 | loop fusion | flops 24116992 | bytes 883712 | tf_op jit(solution)/shard_map/reduce_sum | solution.py:141
  173.8 2.5 psum.14
  176.2 0.2 multiply_reduce_fusion
  176.4 2.5 psum.15
  178.9 0.3 multiply_convert_fusion
  179.2 66.3 %all-gather.11.cloned.1.call-done = bf16[1024,2048]{1,0:T(8,128)(2,1)} async-done(((bf16[1024,512]{1,0:T(8,128)(2,1)}), bf16[1024,2048]{1,0:T(8,128)(2,1)}) %all-gather.11.cloned.1.call-update) | async-done | bytes 4194320 | tf_op jit(solution)/shard_map/all_gather | solution.py:156
  245.5 4.5 %convolution_convert_fusion = bf16[256,2048]{1,0:T(8,128)(2,1)} fusion(bf16[1024,2048]{1,0:T(8,128)(2,1)} %all-gather.11.cloned.1.call-done, bf16[256,512]{1,0:T(8,128)(2,1)S(1)} %multiply_convert_fusion, bf16[256,512]{1,0:T(8,128)(2,1)S(1)} %copy.27), kind=kOutput, calls=%fused_computation.11 | convolution fusion | flops 1075314688 | bytes 5767168 | tf_op jit(solution)/shard_map/dot_general | solution.py:158
  249.9 7.0 %reduce-scatter.2.cloned.1.call-done = bf16[128,2048]{1,0:T(8,128)(2,1)} async-done(((bf16[256,2048]{1,0:T(8,128)(2,1)}), bf16[128,2048]{1,0:T(8,128)(2,1)}) %reduce-scatter.2.cloned.1.call-update) | async-done | bytes 524304 | tf_op jit(solution)/shard_map/reduce_scatter | solution.py:157
  (52 shorter events, 1.3 us)
Async XLA Ops:
  6.5 4.7 %copy-start = (bf16[256,2048]{1,0:T(8,128)(2,1)S(1)}, bf16[256,2048]{1,0:T(8,128)(2,1)}, u32[]{:S(2)}) copy-start(bf16[256,2048]{1,0:T(8,128)(2,1)} %param.14) | copy-start | bytes 3145732
  6.5 5.0 %copy-start.1 = (bf16[512,128]{1,0:T(8,128)(2,1)S(1)}, bf16[512,128]{1,0:T(8,128)(2,1)}, u32[]{:S(2)}) copy-start(bf16[512,128]{1,0:T(8,128)(2,1)} %param.17) | copy-start | bytes 393220
  6.5 28.1 %copy-start.2 = (bf16[512,128]{1,0:T(8,128)(2,1)S(1)}, bf16[512,128]{1,0:T(8,128)(2,1)}, u32[]{:S(2)}) copy-start(bf16[512,128]{1,0:T(8,128)(2,1)} %param.18) | copy-start | bytes 393220
  6.5 64.6 %all-gather.7.cloned.1.call-start = ((), (), s32[]{:S(2)}) async-start(), calls=%async_computation.2 | async-start | bytes 2621440 | tf_op jit(solution)/shard_map/all_gather | solution.py:84
  7.3 111.1 %all-gather.9.cloned.1.call-start = ((), (), s32[]{:S(2)}) async-start(), calls=%async_computation.3 | async-start | bytes 2621440 | tf_op jit(solution)/shard_map/all_gather | solution.py:85
  8.0 48.4 %copy-start.7 = (f32[2048]{0:T(1024)S(1)}, f32[2048]{0:T(1024)}, u32[]{:S(2)}) copy-start(f32[2048]{0:T(1024)} %param.15) | copy-start | bytes 24580
  8.0 156.6 %all-gather.5.cloned.1.call-start = ((), (), s32[]{:S(2)}) async-start(), calls=%async_computation.1 | async-start | bytes 2621440 | tf_op jit(solution)/shard_map/all_gather | solution.py:81
  8.8 236.7 %all-gather.11.cloned.1.call-start = ((), (), s32[]{:S(2)}) async-start(), calls=%async_computation.4 | async-start | bytes 5242880 | tf_op jit(solution)/shard_map/all_gather | solution.py:156
  11.1 49.1 %copy-start.3 = (f32[31,512]{1,0:T(8,128)S(1)}, f32[31,512]{1,0:T(8,128)}, u32[]{:S(2)}) copy-start(f32[31,512]{1,0:T(8,128)} %param.22) | copy-start | bytes 190468
  11.1 49.5 %copy-start.8 = (f32[8]{0:T(128)S(1)}, f32[8]{0:T(128)}, u32[]{:S(2)}) copy-start(f32[8]{0:T(128)} %param.21) | copy-start | bytes 100
  11.2 245.8 %reduce-scatter.2.cloned.1.call-start = ((), (), s32[]{:S(2)}) async-start(), calls=%async_computation.5 | async-start | bytes 1572864 | tf_op jit(solution)/shard_map/reduce_scatter | solution.py:157
  57.4 4.8 %collective-permute-start = (bf16[128,256]{0,1:T(8,128)(2,1)S(1)}, bf16[128,256]{0,1:T(8,128)(2,1)S(1)}, u32[]{:S(2)}, u32[]{:S(2)}) collective-permute-start(bf16[128,256]{0,1:T(8,128)(2,1)S(1)} %get-tuple-element.21), channel_id=1, source_target_pairs={{0,8},{8,16},{16,24},{1,9},{9,17},{17,25},{2,10},{10,18},{18,26},{... | collective-permute-start | bytes 196616 | tf_op jit(solution)/shard_map/ppermute | solution.py:19
  58.9 10.3 %collective-permute-start.1 = (bf16[128,256]{0,1:T(8,128)(2,1)S(1)}, bf16[128,256]{0,1:T(8,128)(2,1)S(1)}, u32[]{:S(2)}, u32[]{:S(2)}) collective-permute-start(bf16[128,256]{0,1:T(8,128)(2,1)S(1)} %get-tuple-element.22), channel_id=1, source_target_pairs={{8,0},{16,8},{24,16},{9,1},{17,9},{25,17},{10,2},{18,10},{26,18},{... | collective-permute-start | bytes 196616 | tf_op jit(solution)/shard_map/ppermute | solution.py:22
  122.1 48.6 %collective-permute-start.2 = (bf16[15,512]{1,0:T(8,128)(2,1)S(1)}, bf16[15,512]{1,0:T(8,128)(2,1)S(1)}, u32[]{:S(2)}, u32[]{:S(2)}) collective-permute-start(bf16[15,512]{1,0:T(8,128)(2,1)S(1)} %get-tuple-element.15), channel_id=1, source_target_pairs={{0,8},{8,16},{16,24},{1,9},{9,17},{17,25},{2,10},{10,18},{18,26},{... | collective-permute-start | bytes 46088 | tf_op jit(solution)/shard_map/ppermute | solution.py:19
  124.2 46.5 %collective-permute-start.3 = (bf16[15,512]{1,0:T(8,128)(2,1)S(1)}, bf16[15,512]{1,0:T(8,128)(2,1)S(1)}, u32[]{:S(2)}, u32[]{:S(2)}) collective-permute-start(bf16[15,512]{1,0:T(8,128)(2,1)S(1)} %get-tuple-element.16), channel_id=1, source_target_pairs={{8,0},{16,8},{24,16},{9,1},{17,9},{25,17},{10,2},{18,10},{26,18},{... | collective-permute-start | bytes 46088 | tf_op jit(solution)/shard_map/ppermute | solution.py:22
  169.2 1.4 copy-start.4
  169.2 9.7 %copy-start.5 = (f32[512]{0:T(512)S(1)}, f32[512]{0:T(512)}, u32[]{:S(2)}) copy-start(f32[512]{0:T(512)} %param.25) | copy-start | bytes 6148
  169.2 9.7 %copy-start.6 = (f32[512]{0:T(512)S(1)}, f32[512]{0:T(512)}, u32[]{:S(2)}) copy-start(f32[512]{0:T(512)} %param.24) | copy-start | bytes 6148
Sparse Core Ops, SparseCore 0:
  8.9 62.1 all-gather.6
  72.7 45.6 all-gather.8
  120.0 44.6 all-gather.4
  166.1 79.3 all-gather.10
  250.1 6.8 reduce-scatter.1
where the time goes:
time: 264 us
  waiting for transfers between devices  172 us (65%)
  blocking collectives  49.7 us (19%)
  between operations  13.5 us (5%)
  matrix products  13.3 us (5%)
  other arithmetic  6.78 us (3%)
  starting transfers between devices  6.35 us (2%)
    all_gather x1, waiting for transfers between devices, local(): own_whole = lax.all_gather(own_rows, 'sp', axis=1, tiled=True)  66.3 us
    all_gather x1, waiting for transfers between devices, local(): piece_gate = lax.all_gather(w_conv_gate, 'sp', axis=0, tiled=True)  47.3 us
    all_gather x1, waiting for transfers between devices, local(): piece_query = lax.all_gather(w_query, 'sp', axis=0, tiled=True)  39.2 us
    all_gather x1, blocking collectives, local(): piece_key = lax.all_gather(w_key, 'sp', axis=0, tiled=True)  23.1 us
    all_gather x1, blocking collectives, local(): piece_value = lax.all_gather(w_value, 'sp', axis=0, tiled=True)  21.7 us
    reduce_scatter x1, waiting for transfers between devices, local(): lax.psum_scatter(jnp.dot(features, own_whole, preferred_element_type=jnp....  7.04 us
    ppermute x2, waiting for transfers between devices, padded(): lax.ppermute(lax.slice_in_dim(block, 0, width, axis=dim), axis, backward)  6.99 us
  transfers between devices with their start and end apart: 9, of which 7 were waited for; matrix products, arithmetic and copies ran while one was open for 7% of the time, Pallas kernels for 0%

commit v1 on v0

--- a/solution.py
+++ b/solution.py
@@ -79,7 +79,12 @@
     kv_cols = w_key.shape[1]
     chan_cols = w_conv_in.shape[1]
     piece_query = lax.all_gather(w_query, "sp", axis=0, tiled=True)
-    piece_key = lax.all_gather(w_key, "sp", axis=0, tiled=True)
+    ring = [w_key]
+    for hop in range(3):
+        ring.append(lax.ppermute(ring[-1], "sp", [(dev, (dev + 1) % 4) for dev in range(4)]))
+    piece_key = jnp.roll(
+        jnp.concatenate(ring[::-1], axis=0), (lax.axis_index("sp") + 1) * ring[0].shape[0], axis=0
+    )
     piece_value = lax.all_gather(w_value, "sp", axis=0, tiled=True)
     piece_conv = lax.all_gather(w_conv_in, "sp", axis=0, tiled=True)
     piece_gate = lax.all_gather(w_conv_gate, "sp", axis=0, tiled=True)

time: 264 us -> 262 us (level)
  blocking collectives: 49.7 us -> 31 us
  waiting for transfers between devices: 172 us -> 185 us
  starting transfers between devices: 6.35 us -> 10.3 us
    all_gather x1 -> x0, blocking collectives: 23.1 us -> none  [local(): piece_key = lax.all_gather(w_key, 'sp', axis=0, tiled=True)]
    ppermute x0 -> x3, waiting for transfers between devices: none -> 10.2 us  [local(): lax.ppermute(ring[-1], 'sp', [(dev, (dev + 1) % 4) for dev in range(4)])]
    all_gather x1, blocking collectives: 21.7 us -> 26.1 us  [local(): piece_value = lax.all_gather(w_value, 'sp', axis=0, tiled=True)]
    all_gather x1, waiting for transfers between devices: 1.88 us -> 5.89 us  [local(): piece_conv = lax.all_gather(w_conv_in, 'sp', axis=0, tiled=True)]
    ppermute x0 -> x3, starting transfers between devices: none -> 3.11 us  [local(): lax.ppermute(ring[-1], 'sp', [(dev, (dev + 1) % 4) for dev in range(4)])]
  transfers between devices with their start and end apart: 9 -> 12, of which waited for: 7 -> 9; matrix products, arithmetic and copies ran while one was open for 7% -> 7% of each run, Pallas kernels for 0% -> 0%
where the time goes in v1:
time: 262 us
  waiting for transfers between devices  185 us (71%)
  blocking collectives  31 us (12%)
  between operations  13.6 us (5%)
  matrix products  13.4 us (5%)
  starting transfers between devices  10.3 us (4%)
  other arithmetic  6.78 us (3%)
    all_gather x1, waiting for transfers between devices, local(): own_whole = lax.all_gather(own_rows, 'sp', axis=1, tiled=True)  66.2 us
    all_gather x1, waiting for transfers between devices, local(): piece_gate = lax.all_gather(w_conv_gate, 'sp', axis=0, tiled=True)  45.6 us
    all_gather x1, waiting for transfers between devices, local(): piece_query = lax.all_gather(w_query, 'sp', axis=0, tiled=True)  39.2 us
    all_gather x1, blocking collectives, local(): piece_value = lax.all_gather(w_value, 'sp', axis=0, tiled=True)  26.1 us
    ppermute x3, waiting for transfers between devices, local(): lax.ppermute(ring[-1], 'sp', [(dev, (dev + 1) % 4) for dev in range(4)])  10.2 us
    reduce_scatter x1, waiting for transfers between devices, local(): lax.psum_scatter(jnp.dot(features, own_whole, preferred_element_type=jnp....  7.04 us
    ppermute x2, waiting for transfers between devices, padded(): lax.ppermute(lax.slice_in_dim(block, 0, width, axis=dim), axis, backward)  7 us
    all_gather x1, waiting for transfers between devices, local(): piece_conv = lax.all_gather(w_conv_in, 'sp', axis=0, tiled=True)  5.89 us
  transfers between devices with their start and end apart: 12, of which 9 were waited for; matrix products, arithmetic and copies ran while one was open for 7% of the time, Pallas kernels for 0%

profile of v1, /device:TPU:0, one launch (start us, length us, event | category | flops | bytes accessed | tf_op | source)
XLA Modules:
  0.0 261.9 jit_solution(3118901343902812022)
XLA Ops:
  6.5 0.7 all-gather.7.cloned.1.call-update
  7.3 0.7 all-gather.9.cloned.1.call-update
  8.1 0.7 all-gather.5.cloned.1.call-update
  8.8 3.1 %collective-permute-start = (bf16[512,128]{1,0:T(8,128)(2,1)}, bf16[512,128]{1,0:T(8,128)(2,1)S(1)}, u32[]{:S(2)}, u32[]{:S(2)}) collective-permute-start(bf16[512,128]{1,0:T(8,128)(2,1)} %param.17), channel_id=1, source_target_pairs={{0,8},{8,16},{16,24},{24,0},{1,9},{9,17},{17,25},{25,1},{2,10},{10... | collective-permute-start | bytes 393224 | tf_op jit(solution)/shard_map/ppermute | solution.py:84
  11.9 1.3 constant_dynamic-slice_fusion
  13.2 1.0 pad_maximum_fusion
  14.7 0.3 fusion.24
  15.0 0.3 fusion.6
  15.2 2.4 collective-permute-done
  17.6 7.8 %collective-permute-done.1 = bf16[512,128]{1,0:T(8,128)(2,1)S(1)} collective-permute-done((bf16[512,128]{1,0:T(8,128)(2,1)S(1)}, bf16[512,128]{1,0:T(8,128)(2,1)S(1)}, u32[]{:S(2)}, u32[]{:S(2)}) %collective-permute-start.1) | collective-permute-done | bytes 131104 | tf_op jit(solution)/shard_map/ppermute | solution.py:84
  25.4 26.1 %all_gather.15 = bf16[2048,128]{1,0:T(8,128)(2,1)S(1)} all-gather(bf16[512,128]{1,0:T(8,128)(2,1)S(1)} %copy-done.2), channel_id=1, replica_groups=mesh['sp'=4,'fs'=4,'tp'=2] {'sp'}, dimensions={0}, use_global_device_ids=true | all-gather | bytes 655360 | tf_op jit(solution)/shard_map/all_gather | solution.py:88
  51.8 0.7 fusion.11
  52.6 2.4 collective-permute-start.3
  54.9 1.3 collective-permute-start.4
  56.4 1.9 collective-permute-done.3
  58.2 7.0 %collective-permute-done.4 = bf16[128,256]{0,1:T(8,128)(2,1)S(1)} collective-permute-done((bf16[128,256]{0,1:T(8,128)(2,1)S(1)}, bf16[128,256]{0,1:T(8,128)(2,1)S(1)}, u32[]{:S(2)}, u32[]{:S(2)}) %collective-permute-start.4) | collective-permute-done | bytes 65568 | tf_op jit(solution)/shard_map/ppermute | solution.py:22
  65.3 5.9 %all-gather.7.cloned.1.call-done = bf16[2048,512]{1,0:T(8,128)(2,1)} async-done(((bf16[512,512]{1,0:T(8,128)(2,1)}), bf16[2048,512]{1,0:T(8,128)(2,1)}) %all-gather.7.cloned.1.call-update) | async-done | bytes 2097168 | tf_op jit(solution)/shard_map/all_gather | solution.py:89
  71.2 45.6 %all-gather.9.cloned.1.call-done = bf16[2048,512]{1,0:T(8,128)(2,1)} async-done(((bf16[512,512]{1,0:T(8,128)(2,1)}), bf16[2048,512]{1,0:T(8,128)(2,1)}) %all-gather.9.cloned.1.call-update) | async-done | bytes 2097168 | tf_op jit(solution)/shard_map/all_gather | solution.py:90
  116.8 3.5 %fusion = f32[256,1024]{1,0:T(8,128)S(1)} fusion(bf16[2048,512]{1,0:T(8,128)(2,1)} %all-gather.9.cloned.1.call-done, bf16[2048,512]{1,0:T(8,128)(2,1)} %all-gather.7.cloned.1.call-done, bf16[256,2048]{1,0:T(8,128)(2,1)S(1)} %copy-done, f32[2048]{0:T(1024)S(1)} %copy-done.7, f32[256]{0:T(256)S(1)} %add_rsqrt_fusion.1), kind=kOutput, calls=%fused_computation | convolution fusion | flops 1084227584 | bytes 6300672 | tf_op jit(solution)/shard_map/dot_general | solution.py:97
  120.5 2.1 collective-permute-start.5
  122.6 1.3 collective-permute-start.6
  123.9 39.2 %all-gather.5.cloned.1.call-done = bf16[2048,512]{1,0:T(8,128)(2,1)} async-done(((bf16[512,512]{1,0:T(8,128)(2,1)}), bf16[2048,512]{1,0:T(8,128)(2,1)}) %all-gather.5.cloned.1.call-update) | async-done | bytes 2097168 | tf_op jit(solution)/shard_map/all_gather | solution.py:81
  163.0 2.6 %fusion.74 = f32[256,512]{0,1:T(8,128)S(1)} fusion(bf16[2048,512]{1,0:T(8,128)(2,1)} %all-gather.5.cloned.1.call-done, bf16[256,2048]{1,0:T(8,128)(2,1)S(1)} %copy-done, f32[2048]{0:T(1024)S(1)} %copy-done.7, f32[256]{0:T(256)S(1)} %add_rsqrt_fusion.1), kind=kOutput, calls=%fused_computation.175 | convolution fusion | flops 538968064 | bytes 3679232 | tf_op jit(solution)/shard_map/dot_general | solution.py:91
  165.8 0.8 fusion.5
  166.7 0.9 fusion.4
  167.7 1.2 fusion.10
  169.1 3.1 %fusion.77 = (f32[256]{0:T(256)S(1)}, f32[256,512]{1,0:T(8,128)S(1)}) fusion(bf16[15,512]{1,0:T(8,128)(2,1)S(1)} %collective-permute-done.6, bf16[256,512]{1,0:T(8,128)(2,1)S(1)} %fusion.22, f32[512]{0:T(512)S(1)} %bitcast.106, f32[512]{0:T(512)S(1)} %bitcast.107, f32[512]{0:T(512)S(1)} %bitcast.78, f32[512]{0:T(512)S(1)} %bitcast.79, f32[512]{0:T(512)S(1)} %bitcast.80, ...), kind=kLoop, calls=%fused_computation.176 | loop fusion | flops 24116992 | bytes 883712 | tf_op jit(solution)/shard_map/reduce_sum | solution.py:146
  172.2 2.5 psum.14
  174.9 2.5 psum.15
  177.6 66.2 %all-gather.11.cloned.1.call-done = bf16[1024,2048]{1,0:T(8,128)(2,1)} async-done(((bf16[1024,512]{1,0:T(8,128)(2,1)}), bf16[1024,2048]{1,0:T(8,128)(2,1)}) %all-gather.11.cloned.1.call-update) | async-done | bytes 4194320 | tf_op jit(solution)/shard_map/all_gather | solution.py:161
  243.9 4.5 %convolution_convert_fusion = bf16[256,2048]{1,0:T(8,128)(2,1)} fusion(bf16[1024,2048]{1,0:T(8,128)(2,1)} %all-gather.11.cloned.1.call-done, bf16[256,512]{1,0:T(8,128)(2,1)S(1)} %multiply_convert_fusion, bf16[256,512]{1,0:T(8,128)(2,1)S(1)} %copy.27), kind=kOutput, calls=%fused_computation.11 | convolution fusion | flops 1075314688 | bytes 5767168 | tf_op jit(solution)/shard_map/dot_general | solution.py:163
  248.4 7.0 %reduce-scatter.2.cloned.1.call-done = bf16[128,2048]{1,0:T(8,128)(2,1)} async-done(((bf16[256,2048]{1,0:T(8,128)(2,1)}), bf16[128,2048]{1,0:T(8,128)(2,1)}) %reduce-scatter.2.cloned.1.call-update) | async-done | bytes 524304 | tf_op jit(solution)/shard_map/reduce_scatter | solution.py:162
  (66 shorter events, 1.9 us)
Async XLA Ops:
  6.5 7.9 %copy-start.3 = (f32[31,512]{1,0:T(8,128)S(1)}, f32[31,512]{1,0:T(8,128)}, u32[]{:S(2)}) copy-start(f32[31,512]{1,0:T(8,128)} %param.22) | copy-start | bytes 190468
  6.5 8.4 %copy-start = (bf16[256,2048]{1,0:T(8,128)(2,1)S(1)}, bf16[256,2048]{1,0:T(8,128)(2,1)}, u32[]{:S(2)}) copy-start(bf16[256,2048]{1,0:T(8,128)(2,1)} %param.14) | copy-start | bytes 3145732
  6.5 18.9 %copy-start.2 = (bf16[512,128]{1,0:T(8,128)(2,1)S(1)}, bf16[512,128]{1,0:T(8,128)(2,1)}, u32[]{:S(2)}) copy-start(bf16[512,128]{1,0:T(8,128)(2,1)} %param.18) | copy-start | bytes 393220
  6.5 64.6 %all-gather.7.cloned.1.call-start = ((), (), s32[]{:S(2)}) async-start(), calls=%async_computation.2 | async-start | bytes 2621440 | tf_op jit(solution)/shard_map/all_gather | solution.py:89
  7.3 109.5 %all-gather.9.cloned.1.call-start = ((), (), s32[]{:S(2)}) async-start(), calls=%async_computation.3 | async-start | bytes 2621440 | tf_op jit(solution)/shard_map/all_gather | solution.py:90
  8.0 43.6 %copy-start.1 = (bf16[512,128]{1,0:T(8,128)(2,1)S(1)}, bf16[512,128]{1,0:T(8,128)(2,1)}, u32[]{:S(2)}) copy-start(bf16[512,128]{1,0:T(8,128)(2,1)} %param.17) | copy-start | bytes 393220
  8.0 155.0 %all-gather.5.cloned.1.call-start = ((), (), s32[]{:S(2)}) async-start(), calls=%async_computation.1 | async-start | bytes 2621440 | tf_op jit(solution)/shard_map/all_gather | solution.py:81
  8.8 235.1 %all-gather.11.cloned.1.call-start = ((), (), s32[]{:S(2)}) async-start(), calls=%async_computation.4 | async-start | bytes 5242880 | tf_op jit(solution)/shard_map/all_gather | solution.py:161
  8.8 8.8 %collective-permute-start = (bf16[512,128]{1,0:T(8,128)(2,1)}, bf16[512,128]{1,0:T(8,128)(2,1)S(1)}, u32[]{:S(2)}, u32[]{:S(2)}) collective-permute-start(bf16[512,128]{1,0:T(8,128)(2,1)} %param.17), channel_id=1, source_target_pairs={{0,8},{8,16},{16,24},{24,0},{1,9},{9,17},{17,25},{25,1},{2,10},{10... | collective-permute-start | bytes 393224 | tf_op jit(solution)/shard_map/ppermute | solution.py:84
  13.2 38.6 %copy-start.7 = (f32[2048]{0:T(1024)S(1)}, f32[2048]{0:T(1024)}, u32[]{:S(2)}) copy-start(f32[2048]{0:T(1024)} %param.15) | copy-start | bytes 24580
  14.3 241.1 %reduce-scatter.2.cloned.1.call-start = ((), (), s32[]{:S(2)}) async-start(), calls=%async_computation.5 | async-start | bytes 1572864 | tf_op jit(solution)/shard_map/reduce_scatter | solution.py:162
  17.6 7.8 %collective-permute-start.1 = (bf16[512,128]{1,0:T(8,128)(2,1)S(1)}, bf16[512,128]{1,0:T(8,128)(2,1)S(1)}, u32[]{:S(2)}, u32[]{:S(2)}) collective-permute-start(bf16[512,128]{1,0:T(8,128)(2,1)S(1)} %collective-permute-done), channel_id=1, source_target_pairs={{0,8},{8,16},{16,24},{24,0},{1,9},{9,17},{17,25},{25,1},{2,10},{10... | collective-permute-start | bytes 393224 | tf_op jit(solution)/shard_map/ppermute | solution.py:84
  25.4 26.1 %collective-permute-start.2 = (bf16[512,128]{1,0:T(8,128)(2,1)S(1)}, bf16[512,128]{1,0:T(8,128)(2,1)S(1)}, u32[]{:S(2)}, u32[]{:S(2)}) collective-permute-start(bf16[512,128]{1,0:T(8,128)(2,1)S(1)} %collective-permute-done.1), channel_id=1, source_target_pairs={{0,8},{8,16},{16,24},{24,0},{1,9},{9,17},{17,25},{25,1},{2,10},{10... | collective-permute-start | bytes 393224 | tf_op jit(solution)/shard_map/ppermute | solution.py:84
  51.5 4.8 %copy-start.8 = (f32[8]{0:T(128)S(1)}, f32[8]{0:T(128)}, u32[]{:S(2)}) copy-start(f32[8]{0:T(128)} %param.21) | copy-start | bytes 100
  52.6 5.7 %collective-permute-start.3 = (bf16[128,256]{0,1:T(8,128)(2,1)S(1)}, bf16[128,256]{0,1:T(8,128)(2,1)S(1)}, u32[]{:S(2)}, u32[]{:S(2)}) collective-permute-start(bf16[128,256]{0,1:T(8,128)(2,1)S(1)} %get-tuple-element.21), channel_id=1, source_target_pairs={{0,8},{8,16},{16,24},{1,9},{9,17},{17,25},{2,10},{10,18},{18,26},{... | collective-permute-start | bytes 196616 | tf_op jit(solution)/shard_map/ppermute | solution.py:19
  54.9 10.3 %collective-permute-start.4 = (bf16[128,256]{0,1:T(8,128)(2,1)S(1)}, bf16[128,256]{0,1:T(8,128)(2,1)S(1)}, u32[]{:S(2)}, u32[]{:S(2)}) collective-permute-start(bf16[128,256]{0,1:T(8,128)(2,1)S(1)} %get-tuple-element.22), channel_id=1, source_target_pairs={{8,0},{16,8},{24,16},{9,1},{17,9},{25,17},{10,2},{18,10},{26,18},{... | collective-permute-start | bytes 196616 | tf_op jit(solution)/shard_map/ppermute | solution.py:22
  120.5 48.6 %collective-permute-start.5 = (bf16[15,512]{1,0:T(8,128)(2,1)S(1)}, bf16[15,512]{1,0:T(8,128)(2,1)S(1)}, u32[]{:S(2)}, u32[]{:S(2)}) collective-permute-start(bf16[15,512]{1,0:T(8,128)(2,1)S(1)} %get-tuple-element.15), channel_id=1, source_target_pairs={{0,8},{8,16},{16,24},{1,9},{9,17},{17,25},{2,10},{10,18},{18,26},{... | collective-permute-start | bytes 46088 | tf_op jit(solution)/shard_map/ppermute | solution.py:19
  122.6 46.5 %collective-permute-start.6 = (bf16[15,512]{1,0:T(8,128)(2,1)S(1)}, bf16[15,512]{1,0:T(8,128)(2,1)S(1)}, u32[]{:S(2)}, u32[]{:S(2)}) collective-permute-start(bf16[15,512]{1,0:T(8,128)(2,1)S(1)} %get-tuple-element.16), channel_id=1, source_target_pairs={{8,0},{16,8},{24,16},{9,1},{17,9},{25,17},{10,2},{18,10},{26,18},{... | collective-permute-start | bytes 46088 | tf_op jit(solution)/shard_map/ppermute | solution.py:22
  167.6 1.4 copy-start.4
  167.6 9.7 %copy-start.5 = (f32[512]{0:T(512)S(1)}, f32[512]{0:T(512)}, u32[]{:S(2)}) copy-start(f32[512]{0:T(512)} %param.25) | copy-start | bytes 6148
  167.6 9.7 %copy-start.6 = (f32[512]{0:T(512)S(1)}, f32[512]{0:T(512)}, u32[]{:S(2)}) copy-start(f32[512]{0:T(512)} %param.24) | copy-start | bytes 6148
Sparse Core Ops, SparseCore 0:
  8.9 62.2 all-gather.6
  72.7 43.9 all-gather.8
  118.4 44.6 all-gather.4
  164.5 79.3 all-gather.10
  248.5 6.8 reduce-scatter.1
